TPU v7x, 32 devices: a whole 2x2x4 slice. The times are simulated.
32 devices in a mesh: fs: 8 (over z, y), tp: 4 (over x, core).
Axes of the slice: x: 2, y: 2, z: 4, core: 2. Of those that a mesh axis runs over, the one named last changes fastest.
Arguments:
- layer_input: bfloat16 [6144, 2048], P('fs', 'tp'), may hold values from -6 to 6
- out_cotangent: bfloat16 [6144, 2048], P('fs', 'tp'), may hold values from -6 to 6
- gate_matrix: bfloat16 [2048, 6144], P('fs', 'tp'), may hold values from -0.125 to 0.125
- up_matrix: bfloat16 [2048, 6144], P('fs', 'tp'), may hold values from -0.125 to 0.125
- down_matrix: bfloat16 [6144, 2048], P('tp', 'fs'), may hold values from -0.078125 to 0.078125
Outputs:
- input_grad: bfloat16 [6144, 2048], P('fs', 'tp')
- gate_grad: float32 [2048, 6144], P('fs', 'tp')
- up_grad: float32 [2048, 6144], P('fs', 'tp')
- down_grad: float32 [6144, 2048], P('tp', 'fs')
All inputs are finite; a program needn't handle non-finite values.
Results may differ from a plain program's by a relative error of at most 0.014.
Values may be sent and summed in bfloat16 or wider, within the bound.
A program may use at most 128 MiB of HBM per device.

v0:
```python
import functools

import jax
import jax.numpy as jnp
from jax import lax
from jax.experimental import pallas as pl
from jax.experimental.pallas import tpu as pltpu
from jax.sharding import PartitionSpec as P

CORES = 2
TILE = 256
STRIPS = 3

NN = ((1,), (0,))
TN = ((0,), (0,))
NT = ((1,), (1,))

GATE, UP, DOWN = range(3)


def dot(left, right, dims):
    return lax.dot_general(left, right, (dims, ((), ())), preferred_element_type=jnp.float32)


def narrow(value):
    return value.astype(jnp.bfloat16)


def wide(value):
    return value.astype(jnp.float32)


def xor(left, right, n):
    total = 0
    k = 1
    while k < n:
        total = total + k * lax.rem(lax.div(left, k) + right // k % 2, 2)
        k *= 2
    return total


def kernel(
    n_fs,
    n_tp,
    layer_input,
    out_cotangent,
    gate_matrix,
    up_matrix,
    down_matrix,
    input_grad,
    gate_grad,
    up_grad,
    down_grad,
    xg,
    w,
    ab,
    delta,
    y_out,
    y_in,
    far_in,
    near_in,
    core_in,
    dx_out,
    dx_core,
    dx_x,
    dx_z,
    local_sem,
    out_sem,
    ag_core,
    ag_near,
    ag_far,
    ag_y,
    tok_z,
    tok_x,
    tok_core,
    rs_y,
    rs_far,
    rs_near,
    rs_core,
    dx_core_sem,
    dx_x_sem,
    dx_z_sem,
):
    n_x = n_tp // CORES
    n_y = n_x
    n_z = n_fs // n_y
    per_quarter = n_fs // n_tp
    far = range(2, n_z, 2)
    tokens, part = layer_input.shape
    depth, width = gate_matrix.shape
    half = width // 2
    model = n_tp * part
    rows = 2 * tokens
    near = n_x * part

    fs = lax.axis_index("fs")
    tp = lax.axis_index("tp")
    z, y = lax.div(fs, n_y), lax.rem(fs, n_y)
    x, core = lax.div(tp, CORES), lax.rem(tp, CORES)
    mine = 1 - lax.rem(lax.rem(z, 2) + core, 2)

    def at_z(by):
        return {"fs": xor(z, by, n_z) * n_y + y}

    def at_y(by):
        return {"fs": z * n_y + xor(y, by, n_y)}

    def at_x(by):
        return {"tp": xor(x, by, n_x) * CORES + core}

    at_core = {"tp": x * CORES + 1 - core}

    def place(zr, yr):
        return xor(z, zr, n_z) * n_y + xor(y, yr, n_y)

    def first(where, tp_there=tp):
        quarter = lax.div(where, per_quarter)
        turned = 0
        k = 1
        while k < n_tp:
            turned = turned + k * lax.rem(lax.div(quarter, k) + lax.div(tp_there, k), 2)
            k *= 2
        slot = lax.rem(turned, CORES) * n_x + lax.div(turned, CORES)
        return slot * part + lax.rem(where, per_quarter) * depth

    def span(start, size):
        return pl.ds(pl.multiple_of(start, depth), size)

    def remote(src, dst, sems, index, device):
        return pltpu.make_async_remote_copy(
            src_ref=src,
            dst_ref=dst,
            send_sem=sems.at[(0, *index)],
            recv_sem=sems.at[(1, *index)],
            device_id=device,
            device_id_type=pl.DeviceIdType.MESH,
        )

    barrier = pltpu.get_barrier_semaphore()
    partners = (
        [at_core, at_z(1)]
        + [at_z(e) for e in far]
        + [at_y(d) for d in range(1, n_y)]
        + [at_x(d) for d in range(1, n_x)]
    )
    for partner in partners:
        pl.semaphore_signal(
            barrier, inc=1, device_id=partner, device_id_type=pl.DeviceIdType.MESH
        )

    shards = (gate_matrix, up_matrix, down_matrix)
    sources = (layer_input, out_cotangent)
    here = first(fs)
    kept_row = mine * here + (1 - mine) * model
    sent_row = mine * first(fs, x * CORES + 1 - core) + (1 - mine) * model

    def keep_shard(m):
        return pltpu.make_async_copy(
            shards[m].at[:, span(core * half, half)],
            w.at[m, span(kept_row, depth), :],
            local_sem.at[m],
        )

    def keep_tokens(k):
        return pltpu.make_async_copy(
            sources[k], xg.at[k, pl.ds(0, tokens), pl.ds(0, part)], local_sem.at[3 + k]
        )

    def swap_shard(m):
        return remote(
            shards[m].at[:, span((1 - core) * half, half)],
            w.at[m, span(sent_row, depth), :],
            ag_core,
            (m,),
            at_core,
        )

    def near_shard(m):
        return remote(
            w.at[m, pl.ds(model, depth), :], w.at[m, span(here, depth), :], ag_near, (m,), at_z(1)
        )

    def far_shard(m, e, s):
        block = w.at[m, span(first(place(s, 0)), depth), :]
        return remote(block, block, ag_far, (m, e - 2 + s), at_z(e))

    def y_shard(m, zr, yr):
        block = w.at[m, span(first(place(zr, 0)), depth), :]
        return remote(block, block, ag_y, (m, zr, yr - 1), at_y(yr))

    def token_z(k):
        return remote(
            sources[k], xg.at[k, pl.ds(tokens, tokens), pl.ds(0, part)], tok_z, (k,), at_z(1)
        )

    def token_x(k, p, xr):
        src = xg.at[k, pl.ds(tokens, tokens), pl.ds(0, part)] if p else sources[k]
        dst = xg.at[k, pl.ds(p * tokens, tokens), pl.ds(xr * part, part)]
        return remote(src, dst, tok_x, (k, p, xr - 1), at_x(xr))

    def token_core(k):
        return remote(
            xg.at[k, :, pl.ds(0, near)], xg.at[k, :, pl.ds(near, near)], tok_core, (k,), at_core
        )

    def send_y_shards(m, zr):
        for yr in range(1, n_y):
            y_shard(m, zr, yr).start()

    for m in range(3):
        keep_shard(m).start()
    for k in range(2):
        keep_tokens(k).start()
    pl.semaphore_wait(barrier, len(partners))

    for m in range(3):
        swap_shard(m).start()
    for k in range(2):
        for xr in range(1, n_x):
            token_x(k, 0, xr).start()
    for m in (GATE, UP):
        keep_shard(m).wait()
        swap_shard(m).wait_recv()
        near_shard(m).start()
        send_y_shards(m, 0)
    token_z(0).start()
    for m in (GATE, UP):
        for e in far:
            far_shard(m, e, 0).start()
    keep_shard(DOWN).wait()
    swap_shard(DOWN).wait_recv()
    send_y_shards(DOWN, 0)
    for m in (GATE, UP):
        near_shard(m).wait_recv()
        for e in far:
            far_shard(m, e, 1).start()
        send_y_shards(m, 1)
    token_z(1).start()
    near_shard(DOWN).start()
    token_z(0).wait_recv()
    for xr in range(1, n_x):
        token_x(0, 1, xr).start()
    for m in (GATE, UP):
        for e in far:
            far_shard(m, e, 0).wait_recv()
            send_y_shards(m, e)
    for e in far:
        far_shard(DOWN, e, 0).start()
    keep_tokens(0).wait()
    for p in range(2):
        for xr in range(1, n_x):
            token_x(0, p, xr).wait_recv()
    token_core(0).start()
    for m in (GATE, UP):
        for e in far:
            far_shard(m, e, 1).wait_recv()
            send_y_shards(m, e + 1)

    def arrived(m):
        for zr in range(n_z):
            for yr in range(1, n_y):
                y_shard(m, zr, yr).wait_recv()

    arrived(GATE)
    arrived(UP)
    token_core(0).wait_recv()

    def tile_of(i):
        return pl.ds(pl.multiple_of(i * TILE, TILE), TILE)

    strips = [slice(s * half // STRIPS, (s + 1) * half // STRIPS) for s in range(STRIPS)]

    def first_stage(begin, end):
        @pl.loop(begin, end)
        def _(i):
            tile = tile_of(i)
            mine_rows = xg[0, tile, :]
            for cols in strips:
                gate_pre = dot(mine_rows, w[GATE, :model, cols], NN)
                up_pre = dot(mine_rows, w[UP, :model, cols], NN)
                sigmoid_gate = jax.nn.sigmoid(gate_pre)
                activation = gate_pre * sigmoid_gate
                ab[0, tile, cols] = activation
                ab[1, tile, cols] = up_pre * sigmoid_gate * (1.0 + gate_pre * (1.0 - sigmoid_gate))
                delta[DOWN, tile, cols] = narrow(activation * up_pre)

    tiles = rows // TILE
    first_stage(0, tiles // 3)
    token_z(1).wait_recv()
    for xr in range(1, n_x):
        token_x(1, 1, xr).start()
    first_stage(tiles // 3, 2 * tiles // 3)
    near_shard(DOWN).wait_recv()
    for e in far:
        far_shard(DOWN, e, 1).start()
    send_y_shards(DOWN, 1)
    first_stage(2 * tiles // 3, tiles)
    keep_tokens(1).wait()
    for p in range(2):
        for xr in range(1, n_x):
            token_x(1, p, xr).wait_recv()
    token_core(1).start()
    for e in far:
        far_shard(DOWN, e, 0).wait_recv()
        send_y_shards(DOWN, e)
    token_core(1).wait_recv()

    def term(m, zr, yr):
        cols = span(first(place(zr, yr)), depth)
        pieces = [pl.ds(p * tokens, tokens) for p in range(2)]
        return sum(dot(xg[lax.div(m, 2), piece, cols], delta[m, piece, :], TN) for piece in pieces)

    def y_term(m, zr, yr):
        return remote(
            y_out.at[m, zr, yr - 1], y_in.at[m, zr, yr - 1], rs_y, (m, zr, yr - 1), at_y(yr)
        )

    def far_sum(m, zr, e):
        return remote(y_out.at[m, zr, 0], far_in.at[m, zr - 2], rs_far, (m, zr - 2), at_z(e))

    def near_sum(m):
        return remote(y_out.at[m, 1, 0], near_in.at[m], rs_near, (m,), at_z(1))

    def core_sum(m):
        return remote(y_out.at[m, 0, 0], core_in.at[m], rs_core, (m,), at_core)

    def send_y(m, zr):
        for yr in range(1, n_y):
            y_out[m, zr, yr - 1] = narrow(term(m, zr, yr))
            y_term(m, zr, yr).start()

    def y_sum(m, zr):
        total = term(m, zr, 0)
        for yr in range(1, n_y):
            y_term(m, zr, yr).wait_recv()
            total = total + wide(y_in[m, zr, yr - 1])
        y_term(m, zr, 1).wait_send()
        return total

    def cross(m, zr, e):
        y_out[m, zr, 0] = narrow(y_sum(m, zr))
        far_sum(m, zr, e).start()

    def pair(m):
        total = y_sum(m, 1)
        for e in far:
            far_sum(m, e + 1, e).wait_recv()
            total = total + wide(far_in[m, e - 1])
        y_out[m, 1, 0] = narrow(total)
        near_sum(m).start()

    def own_stage(m):
        return pl.ds(pl.multiple_of((2 * m + core) * depth, depth), depth)

    def other_stage(m):
        return pl.ds(pl.multiple_of((2 * m + 1 - core) * depth, depth), depth)

    def own(m):
        total = y_sum(m, 0)
        for e in far:
            far_sum(m, e, e).wait_recv()
            total = total + wide(far_in[m, e - 2])
        near_sum(m).wait_recv()
        other = wide(near_in[m])
        y_out[m, 0, 0] = narrow(jnp.where(mine == 1, other, total))
        core_sum(m).start()
        ab[0, own_stage(m), :] = jnp.where(mine == 1, total, other)

    def put(m):
        out = (gate_grad, up_grad, down_grad)[m]
        return [
            pltpu.make_async_copy(
                ab.at[0, pl.ds((2 * m + p) * depth, depth), :],
                out.at[:, pl.ds(p * half, half)],
                out_sem.at[m, p],
            )
            for p in range(2)
        ]

    def finish(m):
        core_sum(m).wait_recv()
        ab[0, other_stage(m), :] = wide(core_in[m])
        for copy in put(m):
            copy.start()

    @pl.loop(0, n_z - 2)
    def _(i):
        send_y(DOWN, n_z - 1 - i)

    for e in far:
        far_shard(DOWN, e, 1).wait_recv()
        send_y_shards(DOWN, e + 1)
    arrived(DOWN)

    def second_stage(begin, end):
        @pl.loop(begin, end)
        def _(i):
            tile = tile_of(i)
            mine_rows = xg[1, tile, :]
            for cols in strips:
                hidden_delta = dot(mine_rows, w[DOWN, :model, cols], NN)
                delta[UP, tile, cols] = narrow(hidden_delta * ab[0, tile, cols])
                delta[GATE, tile, cols] = narrow(hidden_delta * ab[1, tile, cols])

    second_stage(0, tiles)

    @pl.loop(0, 2 * (n_z - 2))
    def _(i):
        send_y(lax.rem(i, 2), n_z - 1 - lax.div(i, 2))

    for e in far:
        for s in (1, 0):
            cross(DOWN, e + s, e)

    @pl.loop(0, 2)
    def _(i):
        send_y(DOWN, 1 - i)

    @pl.loop(0, 4)
    def _(i):
        send_y(lax.rem(i, 2), 1 - lax.div(i, 2))

    for e in far:

        @pl.loop(0, 2)
        def _(m):
            cross(m, e + 1, e)

    def dx_tile(tile, begin):
        total = dot(delta[GATE, tile, :], w[GATE, begin : begin + part, :], NT)
        return total + dot(delta[UP, tile, :], w[UP, begin : begin + part, :], NT)

    dx_swap = remote(dx_out, dx_core, dx_core_sem, (), at_core)

    @pl.loop(0, tiles)
    def _(i):
        tile = tile_of(i)
        for xr in range(n_x):
            cols = pl.ds(xr * part, part)
            dx_out[tile, cols] = narrow(dx_tile(tile, near + xr * part))

    dx_swap.start()

    for e in far:

        @pl.loop(0, 2)
        def _(m):
            cross(m, e, e)

    dx_swap.wait_recv()

    @pl.loop(0, tiles)
    def _(i):
        tile = tile_of(i)
        for xr in range(n_x):
            cols = pl.ds(xr * part, part)
            dx_core[tile, cols] = narrow(dx_tile(tile, xr * part) + wide(dx_core[tile, cols]))

    def dx_over_x(xr):
        return remote(
            dx_core.at[:, pl.ds(xr * part, part)], dx_x.at[xr - 1], dx_x_sem, (xr - 1,), at_x(xr)
        )

    for xr in range(1, n_x):
        dx_over_x(xr).start()

    pair(DOWN)
    own(DOWN)
    finish(DOWN)

    for xr in range(1, n_x):
        dx_over_x(xr).wait_recv()

    @pl.loop(0, tiles)
    def _(i):
        tile = tile_of(i)
        total = wide(dx_core[tile, pl.ds(0, part)])
        for xr in range(1, n_x):
            total = total + wide(dx_x[xr - 1, tile, :])
        dx_core[tile, pl.ds(0, part)] = narrow(total)

    dx_over_z = remote(
        dx_core.at[pl.ds(tokens, tokens), pl.ds(0, part)], dx_z, dx_z_sem, (), at_z(1)
    )
    dx_over_z.start()

    @pl.loop(0, 2)
    def _(m):
        pair(m)

    dx_over_z.wait_recv()

    @pl.loop(0, tokens // TILE)
    def _(i):
        tile = tile_of(i)
        dx_z[tile, :] = narrow(wide(dx_core[tile, pl.ds(0, part)]) + wide(dx_z[tile, :]))

    put_dx = pltpu.make_async_copy(dx_z, input_grad, local_sem.at[5])
    put_dx.start()

    @pl.loop(0, 2)
    def _(m):
        own(m)

    for m in (GATE, UP):
        finish(m)

    dx_swap.wait_send()
    dx_over_z.wait_send()
    for xr in range(1, n_x):
        dx_over_x(xr).wait_send()
    for k in range(2):
        token_z(k).wait_send()
        token_core(k).wait_send()
        for p in range(2):
            for xr in range(1, n_x):
                token_x(k, p, xr).wait_send()
    for m in range(3):
        swap_shard(m).wait_send()
        near_shard(m).wait_send()
        near_sum(m).wait_send()
        core_sum(m).wait_send()
        for e in far:
            for s in range(2):
                far_shard(m, e, s).wait_send()
                far_sum(m, e + s, e).wait_send()
        for zr in range(n_z):
            for yr in range(1, n_y):
                y_shard(m, zr, yr).wait_send()
                if yr > 1:
                    y_term(m, zr, yr).wait_send()
        for copy in put(m):
            copy.wait()
    put_dx.wait()


def make(n_fs, n_tp):
    n_x = n_tp // CORES
    n_y = n_x
    n_z = n_fs // n_y

    def on_device(layer_input, out_cotangent, gate_matrix, up_matrix, down_matrix):
        tokens, part = layer_input.shape
        depth, width = gate_matrix.shape
        half = width // 2
        model = n_tp * part
        rows = 2 * tokens
        near = n_x * part
        bf16, f32 = jnp.bfloat16, jnp.float32
        sem = pltpu.SemaphoreType.DMA
        any_space = pl.BlockSpec(memory_space=pl.ANY)
        wide_grad = jax.ShapeDtypeStruct((depth, width), f32)
        flops = 2 * 8 * rows * half * model
        input_grad, gate_grad, up_grad, down_grad = pl.pallas_call(
            functools.partial(kernel, n_fs, n_tp),
            out_shape=(
                jax.ShapeDtypeStruct((tokens, part), bf16),
                wide_grad,
                wide_grad,
                wide_grad,
            ),
            in_specs=[any_space] * 5,
            out_specs=(any_space,) * 4,
            scratch_shapes=[
                pltpu.VMEM((2, rows, model), bf16),
                pltpu.VMEM((3, model + depth, half), bf16),
                pltpu.VMEM((2, rows, half), f32),
                pltpu.VMEM((3, rows, half), bf16),
                pltpu.VMEM((3, n_z, n_y - 1, depth, half), bf16),
                pltpu.VMEM((3, n_z, n_y - 1, depth, half), bf16),
                pltpu.VMEM((3, n_z - 2, depth, half), bf16),
                pltpu.VMEM((3, depth, half), bf16),
                pltpu.VMEM((3, depth, half), bf16),
                pltpu.VMEM((rows, near), bf16),
                pltpu.VMEM((rows, near), bf16),
                pltpu.VMEM((n_x - 1, rows, part), bf16),
                pltpu.VMEM((tokens, part), bf16),
                sem((6,)),
                sem((3, 2)),
                sem((2, 3)),
                sem((2, 3)),
                sem((2, 3, n_z - 2)),
                sem((2, 3, n_z, n_y - 1)),
                sem((2, 2)),
                sem((2, 2, 2, n_x - 1)),
                sem((2, 2)),
                sem((2, 3, n_z, n_y - 1)),
                sem((2, 3, n_z - 2)),
                sem((2, 3)),
                sem((2, 3)),
                sem((2,)),
                sem((2, n_x - 1)),
                sem((2,)),
            ],
            compiler_params=pltpu.CompilerParams(
                collective_id=0, has_side_effects=True, vmem_limit_bytes=67043328
            ),
            cost_estimate=pl.CostEstimate(
                flops=flops, bytes_accessed=rows * model, transcendentals=rows * half
            ),
        )(layer_input, out_cotangent, gate_matrix, up_matrix, down_matrix.T)
        return input_grad, gate_grad, up_grad, down_grad.T

    return on_device


def solution(mesh):
    return jax.shard_map(
        make(mesh.shape["fs"], mesh.shape["tp"]),
        mesh=mesh,
        in_specs=(P("fs", "tp"), P("fs", "tp"), P("fs", "tp"), P("fs", "tp"), P("tp", "fs")),
        out_specs=(P("fs", "tp"), P("fs", "tp"), P("fs", "tp"), P("tp", "fs")),
        check_vma=False,
    )
```

profile of v0, /device:TPU:3, one launch (start us, length us, event | category | flops | bytes accessed | tf_op | source)
XLA Modules:
  0.0 308.0 jit_solution(15081054323111789982)
XLA Ops:
  0.6 2.3 copy.9
  2.9 297.2 %shard_map.84 = (bf16[768,512]{1,0:T(8,128)(2,1)}, f32[256,1536]{1,0:T(8,128)}, f32[256,1536]{1,0:T(8,128)}, f32[256,1536]{1,0:T(8,128)}) custom-call(bf16[768,512]{1,0:T(8,128)(2,1)} %layer_input.1, bf16[768,512]{1,0:T(8,128)(2,1)} %out_cotangent.1, bf16[256,1536]{1,0:T(8,128)(2,1)} %gate_matrix.1, bf16[256,1536]{1,0:T(8,128)(2,1)} %up_matrix.1, ...), custom_call_target="tpu_custom_call" | custom-call | flops 38654705664 | bytes 3145728 | tf_op jit(solution)/shard_map/pallas_call | solution.py:554
  300.1 0.0 copy-start.2
  300.1 3.1 %copy.10 = f32[1536,256]{1,0:T(8,128)} copy(f32[1536,256]{0,1:T(8,128)} %bitcast.2) | data formatting | bytes 3145728
  303.2 0.0 copy-done.2
  303.2 0.0 copy-start.1
  303.2 0.9 copy.14
  304.1 0.8 copy-done.1
  304.9 0.0 copy-start
  304.9 1.1 copy.15
  306.0 0.8 copy-done
  306.9 1.1 copy.16
Async XLA Ops:
  300.1 3.1 %copy-start.2 = (bf16[768,512]{1,0:T(8,128)(2,1)S(1)}, bf16[768,512]{1,0:T(8,128)(2,1)}, u32[]{:S(2)}) copy-start(bf16[768,512]{1,0:T(8,128)(2,1)} %get-tuple-element.20) | copy-start | bytes 2359300
  303.2 1.7 copy-start.1
  304.9 2.0 copy-start
where the time goes:
time: 308 us
  Pallas kernels  297 us (96%)
  local copies, waits for them, and re-layouts  10.2 us (3%)
    pallas_call x1, Pallas kernels, on_device(): pl.pallas_call(functools.partial(kernel, n_fs, n_tp), out_shape=(jax.Shap...  297 us
    unnamed x11, local copies, waits for them, and re-layouts  10.2 us

commit v1 on v0

--- a/solution.py
+++ b/solution.py
@@ -10,6 +10,8 @@
 CORES = 2
 TILE = 256
 STRIPS = 3
+HALVES = 2
+PIECES = 3
 
 NN = ((1,), (0,))
 TN = ((0,), (0,))
@@ -148,11 +150,21 @@
             barrier, inc=1, device_id=partner, device_id_type=pl.DeviceIdType.MESH
         )
 
-    shards = (gate_matrix, up_matrix, down_matrix)
+    shards = (gate_matrix, up_matrix)
     sources = (layer_input, out_cotangent)
     here = first(fs)
     kept_row = mine * here + (1 - mine) * model
     sent_row = mine * first(fs, x * CORES + 1 - core) + (1 - mine) * model
+
+    def load_down():
+        return pltpu.make_async_copy(
+            down_matrix, dx_core.at[pl.ds(0, width), pl.ds(0, depth)], local_sem.at[DOWN]
+        )
+
+    def turn_down():
+        load_down().wait()
+        w[DOWN, span(kept_row, depth), :] = dx_core[span(core * half, half), :depth].T
+        y_out[DOWN, 0, 0] = dx_core[span((1 - core) * half, half), :depth].T
 
     def keep_shard(m):
         return pltpu.make_async_copy(
@@ -167,8 +179,12 @@
         )
 
     def swap_shard(m):
+        if m == DOWN:
+            src = y_out.at[DOWN, 0, 0]
+        else:
+            src = shards[m].at[:, span((1 - core) * half, half)]
         return remote(
-            shards[m].at[:, span((1 - core) * half, half)],
+            src,
             w.at[m, span(sent_row, depth), :],
             ag_core,
             (m,),
@@ -188,32 +204,78 @@
         block = w.at[m, span(first(place(zr, 0)), depth), :]
         return remote(block, block, ag_y, (m, zr, yr - 1), at_y(yr))
 
-    def token_z(k):
+    piece = tokens // PIECES
+
+    def token_z(k, h):
         return remote(
-            sources[k], xg.at[k, pl.ds(tokens, tokens), pl.ds(0, part)], tok_z, (k,), at_z(1)
+            sources[k].at[pl.ds(h * piece, piece), :],
+            xg.at[k, pl.ds(tokens + h * piece, piece), pl.ds(0, part)],
+            tok_z,
+            (k, h),
+            at_z(1),
         )
 
     def token_x(k, p, xr):
-        src = xg.at[k, pl.ds(tokens, tokens), pl.ds(0, part)] if p else sources[k]
-        dst = xg.at[k, pl.ds(p * tokens, tokens), pl.ds(xr * part, part)]
+        here = pl.ds(tokens + (p - 1) * piece, piece) if p else pl.ds(0, tokens)
+        src = xg.at[k, here, pl.ds(0, part)] if p else sources[k]
+        dst = xg.at[k, here, pl.ds(xr * part, part)]
         return remote(src, dst, tok_x, (k, p, xr - 1), at_x(xr))
 
-    def token_core(k):
+    def token_core(k, p):
+        here = pl.ds(tokens + (p - 1) * piece, piece) if p else pl.ds(0, tokens)
         return remote(
-            xg.at[k, :, pl.ds(0, near)], xg.at[k, :, pl.ds(near, near)], tok_core, (k,), at_core
-        )
+            xg.at[k, here, pl.ds(0, near)],
+            xg.at[k, here, pl.ds(near, near)],
+            tok_core,
+            (k, p),
+            at_core,
+        )
+
+    def pass_tokens(k, h):
+        token_z(k, h).wait_recv()
+        for xr in range(1, n_x):
+            token_x(k, 1 + h, xr).start()
+
+    def join_tokens(k, p):
+        if p == 0:
+            keep_tokens(k).wait()
+        for xr in range(1, n_x):
+            token_x(k, p, xr).wait_recv()
+        token_core(k, p).start()
+
+    def await_tokens(k):
+        for p in range(1 + PIECES):
+            token_core(k, p).wait_recv()
+
+    def relay_near(m):
+        near_shard(m).wait_recv()
+        for e in far:
+            far_shard(m, e, 1).start()
+        send_y_shards(m, 1)
+
+    def relay_far(m, s):
+        for e in far:
+            far_shard(m, e, s).wait_recv()
+            send_y_shards(m, e + s)
+
+    def start_last():
+        for h in range(PIECES):
+            token_z(1, h).start()
+        near_shard(DOWN).start()
+
 
     def send_y_shards(m, zr):
         for yr in range(1, n_y):
             y_shard(m, zr, yr).start()
 
-    for m in range(3):
+    for m in (GATE, UP):
         keep_shard(m).start()
+    load_down().start()
     for k in range(2):
         keep_tokens(k).start()
     pl.semaphore_wait(barrier, len(partners))
 
-    for m in range(3):
+    for m in (GATE, UP):
         swap_shard(m).start()
     for k in range(2):
         for xr in range(1, n_x):
@@ -223,38 +285,47 @@
         swap_shard(m).wait_recv()
         near_shard(m).start()
         send_y_shards(m, 0)
-    token_z(0).start()
+    for h in range(PIECES):
+        token_z(0, h).start()
     for m in (GATE, UP):
         for e in far:
             far_shard(m, e, 0).start()
-    keep_shard(DOWN).wait()
+    turn_down()
+    swap_shard(DOWN).start()
     swap_shard(DOWN).wait_recv()
     send_y_shards(DOWN, 0)
-    for m in (GATE, UP):
-        near_shard(m).wait_recv()
-        for e in far:
-            far_shard(m, e, 1).start()
-        send_y_shards(m, 1)
-    token_z(1).start()
-    near_shard(DOWN).start()
-    token_z(0).wait_recv()
-    for xr in range(1, n_x):
-        token_x(0, 1, xr).start()
-    for m in (GATE, UP):
-        for e in far:
-            far_shard(m, e, 0).wait_recv()
-            send_y_shards(m, e)
+    outer = lax.div(jnp.abs(2 * z - (n_z - 1)), n_z - 1)
+
+    @pl.when(outer == 0)
+    def _():
+        for m in (GATE, UP):
+            relay_near(m)
+        start_last()
+        for h in range(PIECES):
+            pass_tokens(0, h)
+        for m in (GATE, UP):
+            relay_far(m, 0)
+        for p in range(1 + PIECES):
+            join_tokens(0, p)
+        for m in (GATE, UP):
+            relay_far(m, 1)
+
+    @pl.when(outer == 1)
+    def _():
+        for m in (GATE, UP):
+            relay_far(m, 0)
+        for m in (GATE, UP):
+            relay_near(m)
+        for m in (GATE, UP):
+            relay_far(m, 1)
+        start_last()
+        for h in range(PIECES):
+            pass_tokens(0, h)
+            join_tokens(0, h)
+        join_tokens(0, PIECES)
+
     for e in far:
         far_shard(DOWN, e, 0).start()
-    keep_tokens(0).wait()
-    for p in range(2):
-        for xr in range(1, n_x):
-            token_x(0, p, xr).wait_recv()
-    token_core(0).start()
-    for m in (GATE, UP):
-        for e in far:
-            far_shard(m, e, 1).wait_recv()
-            send_y_shards(m, e + 1)
 
     def arrived(m):
         for zr in range(n_z):
@@ -263,7 +334,7 @@
 
     arrived(GATE)
     arrived(UP)
-    token_core(0).wait_recv()
+    await_tokens(0)
 
     def tile_of(i):
         return pl.ds(pl.multiple_of(i * TILE, TILE), TILE)
@@ -285,25 +356,19 @@
                 delta[DOWN, tile, cols] = narrow(activation * up_pre)
 
     tiles = rows // TILE
-    first_stage(0, tiles // 3)
-    token_z(1).wait_recv()
-    for xr in range(1, n_x):
-        token_x(1, 1, xr).start()
-    first_stage(tiles // 3, 2 * tiles // 3)
-    near_shard(DOWN).wait_recv()
-    for e in far:
-        far_shard(DOWN, e, 1).start()
-    send_y_shards(DOWN, 1)
-    first_stage(2 * tiles // 3, tiles)
-    keep_tokens(1).wait()
-    for p in range(2):
-        for xr in range(1, n_x):
-            token_x(1, p, xr).wait_recv()
-    token_core(1).start()
-    for e in far:
-        far_shard(DOWN, e, 0).wait_recv()
-        send_y_shards(DOWN, e)
-    token_core(1).wait_recv()
+    for h in range(PIECES):
+        first_stage(h * tiles // PIECES, (h + 1) * tiles // PIECES)
+        pass_tokens(1, h)
+        join_tokens(1, h)
+        if h == 0:
+
+            @pl.when(outer == 1)
+            def _():
+                relay_far(DOWN, 0)
+
+    relay_near(DOWN)
+    join_tokens(1, PIECES)
+    await_tokens(1)
 
     def term(m, zr, yr):
         cols = span(first(place(zr, yr)), depth)
@@ -364,10 +429,17 @@
         other = wide(near_in[m])
         y_out[m, 0, 0] = narrow(jnp.where(mine == 1, other, total))
         core_sum(m).start()
-        ab[0, own_stage(m), :] = jnp.where(mine == 1, total, other)
+        kept = jnp.where(mine == 1, total, other)
+        if m is DOWN:
+            ab[1, span(core * half, half), :depth] = kept.T
+        else:
+            ab[0, own_stage(m), :] = kept
 
     def put(m):
-        out = (gate_grad, up_grad, down_grad)[m]
+        if m == DOWN:
+            stage = ab.at[1, pl.ds(0, width), pl.ds(0, depth)]
+            return [pltpu.make_async_copy(stage, down_grad, out_sem.at[DOWN, 0])]
+        out = (gate_grad, up_grad)[m]
         return [
             pltpu.make_async_copy(
                 ab.at[0, pl.ds((2 * m + p) * depth, depth), :],
@@ -379,17 +451,33 @@
 
     def finish(m):
         core_sum(m).wait_recv()
-        ab[0, other_stage(m), :] = wide(core_in[m])
+        if m == DOWN:
+            ab[1, span((1 - core) * half, half), :depth] = wide(core_in[m]).T
+        else:
+            ab[0, other_stage(m), :] = wide(core_in[m])
         for copy in put(m):
             copy.start()
 
-    @pl.loop(0, n_z - 2)
+    send_y(DOWN, 3)
+
+    @pl.when(outer == 0)
+    def _():
+        relay_far(DOWN, 0)
+        relay_far(DOWN, 1)
+
+    @pl.when(outer == 1)
+    def _():
+        cross(DOWN, 3, 2)
+        relay_far(DOWN, 1)
+
+    @pl.loop(0, 2)
     def _(i):
-        send_y(DOWN, n_z - 1 - i)
-
-    for e in far:
-        far_shard(DOWN, e, 1).wait_recv()
-        send_y_shards(DOWN, e + 1)
+        send_y(DOWN, 2 - i)
+
+    @pl.when(outer == 0)
+    def _():
+        cross(DOWN, 3, 2)
+
     arrived(DOWN)
 
     def second_stage(begin, end):
@@ -404,90 +492,100 @@
 
     second_stage(0, tiles)
 
-    @pl.loop(0, 2 * (n_z - 2))
-    def _(i):
-        send_y(lax.rem(i, 2), n_z - 1 - lax.div(i, 2))
-
-    for e in far:
-        for s in (1, 0):
-            cross(DOWN, e + s, e)
-
-    @pl.loop(0, 2)
-    def _(i):
-        send_y(DOWN, 1 - i)
-
-    @pl.loop(0, 4)
-    def _(i):
-        send_y(lax.rem(i, 2), 1 - lax.div(i, 2))
-
-    for e in far:
-
-        @pl.loop(0, 2)
-        def _(m):
-            cross(m, e + 1, e)
-
     def dx_tile(tile, begin):
         total = dot(delta[GATE, tile, :], w[GATE, begin : begin + part, :], NT)
         return total + dot(delta[UP, tile, :], w[UP, begin : begin + part, :], NT)
 
-    dx_swap = remote(dx_out, dx_core, dx_core_sem, (), at_core)
-
-    @pl.loop(0, tiles)
-    def _(i):
-        tile = tile_of(i)
-        for xr in range(n_x):
-            cols = pl.ds(xr * part, part)
-            dx_out[tile, cols] = narrow(dx_tile(tile, near + xr * part))
-
-    dx_swap.start()
-
-    for e in far:
-
-        @pl.loop(0, 2)
-        def _(m):
-            cross(m, e, e)
-
-    dx_swap.wait_recv()
-
-    @pl.loop(0, tiles)
-    def _(i):
-        tile = tile_of(i)
-        for xr in range(n_x):
-            cols = pl.ds(xr * part, part)
-            dx_core[tile, cols] = narrow(dx_tile(tile, xr * part) + wide(dx_core[tile, cols]))
-
-    def dx_over_x(xr):
+    def dx_rows(p):
+        return pl.ds(p * tokens, tokens)
+
+    def dx_swap(p):
+        here = dx_rows(p)
+        return remote(dx_out.at[here, :], dx_core.at[here, :], dx_core_sem, (p,), at_core)
+
+    def dx_over_x(p, xr):
+        here = dx_rows(p)
         return remote(
-            dx_core.at[:, pl.ds(xr * part, part)], dx_x.at[xr - 1], dx_x_sem, (xr - 1,), at_x(xr)
-        )
-
-    for xr in range(1, n_x):
-        dx_over_x(xr).start()
-
-    pair(DOWN)
-    own(DOWN)
-    finish(DOWN)
-
-    for xr in range(1, n_x):
-        dx_over_x(xr).wait_recv()
-
-    @pl.loop(0, tiles)
-    def _(i):
-        tile = tile_of(i)
-        total = wide(dx_core[tile, pl.ds(0, part)])
-        for xr in range(1, n_x):
-            total = total + wide(dx_x[xr - 1, tile, :])
-        dx_core[tile, pl.ds(0, part)] = narrow(total)
+            dx_core.at[here, pl.ds(xr * part, part)],
+            dx_x.at[xr - 1, here, :],
+            dx_x_sem,
+            (p, xr - 1),
+            at_x(xr),
+        )
 
     dx_over_z = remote(
         dx_core.at[pl.ds(tokens, tokens), pl.ds(0, part)], dx_z, dx_z_sem, (), at_z(1)
     )
+
+    def dx_tiles(p):
+        return pl.loop(p * tiles // 2, (p + 1) * tiles // 2)
+
+    def dx_give(p):
+        @dx_tiles(p)
+        def _(i):
+            tile = tile_of(i)
+            for xr in range(n_x):
+                cols = pl.ds(xr * part, part)
+                dx_out[tile, cols] = narrow(dx_tile(tile, near + xr * part))
+
+        dx_swap(p).start()
+
+    def dx_take(p):
+        dx_swap(p).wait_recv()
+
+        @dx_tiles(p)
+        def _(i):
+            tile = tile_of(i)
+            for xr in range(n_x):
+                cols = pl.ds(xr * part, part)
+                dx_core[tile, cols] = narrow(dx_tile(tile, xr * part) + wide(dx_core[tile, cols]))
+
+        for xr in range(1, n_x):
+            dx_over_x(p, xr).start()
+
+    def dx_sum(p):
+        for xr in range(1, n_x):
+            dx_over_x(p, xr).wait_recv()
+
+        @dx_tiles(p)
+        def _(i):
+            tile = tile_of(i)
+            total = wide(dx_core[tile, pl.ds(0, part)])
+            for xr in range(1, n_x):
+                total = total + wide(dx_x[xr - 1, tile, :])
+            dx_core[tile, pl.ds(0, part)] = narrow(total)
+
+    def send_pair(zr):
+        @pl.loop(0, 2)
+        def _(m):
+            send_y(m, zr)
+
+    dx_give(1)
+    send_pair(3)
+    cross(DOWN, 2, 2)
+    dx_take(1)
+    pair(DOWN)
+    send_y(GATE, 1)
+    dx_give(0)
+    cross(GATE, 3, 2)
+    send_y(UP, 1)
+    dx_take(0)
+    cross(UP, 3, 2)
+    send_pair(2)
+    dx_sum(1)
     dx_over_z.start()
+    pair(GATE)
+    swap_shard(DOWN).wait_send()
+    send_y(DOWN, 0)
+    send_y(GATE, 0)
+    pair(UP)
+    send_y(UP, 0)
 
     @pl.loop(0, 2)
     def _(m):
-        pair(m)
-
+        cross(m, 2, 2)
+
+    dx_sum(0)
     dx_over_z.wait_recv()
 
     @pl.loop(0, tokens // TILE)
@@ -497,6 +595,8 @@
 
     put_dx = pltpu.make_async_copy(dx_z, input_grad, local_sem.at[5])
     put_dx.start()
+    own(DOWN)
+    finish(DOWN)
 
     @pl.loop(0, 2)
     def _(m):
@@ -505,18 +605,21 @@
     for m in (GATE, UP):
         finish(m)
 
-    dx_swap.wait_send()
     dx_over_z.wait_send()
-    for xr in range(1, n_x):
-        dx_over_x(xr).wait_send()
+    for p in range(2):
+        dx_swap(p).wait_send()
+        for xr in range(1, n_x):
+            dx_over_x(p, xr).wait_send()
     for k in range(2):
-        token_z(k).wait_send()
-        token_core(k).wait_send()
-        for p in range(2):
+        for h in range(PIECES):
+            token_z(k, h).wait_send()
+        for p in range(1 + PIECES):
+            token_core(k, p).wait_send()
             for xr in range(1, n_x):
                 token_x(k, p, xr).wait_send()
     for m in range(3):
-        swap_shard(m).wait_send()
+        if m != DOWN:
+            swap_shard(m).wait_send()
         near_shard(m).wait_send()
         near_sum(m).wait_send()
         core_sum(m).wait_send()
@@ -534,6 +637,44 @@
     put_dx.wait()
 
 
+def hand_over(*refs):
+    count = (len(refs) - 2) // 3
+    sources, results, stages = refs[:count], refs[count : 2 * count], refs[2 * count : 3 * count]
+    came, went = refs[3 * count :]
+
+    def piece(ref, p):
+        size = ref.shape[0] // HALVES
+        return ref.at[pl.ds(p * size, size), :]
+
+    def load(i, p):
+        return pltpu.make_async_copy(piece(sources[i], p), piece(stages[i], p), came.at[i, p])
+
+    def store(i, p):
+        return pltpu.make_async_copy(piece(stages[i], p), piece(results[i], p), went.at[i, p])
+
+    order = [(i, p) for i in range(count) for p in range(HALVES)]
+    for i, p in order:
+        load(i, p).start()
+    for i, p in order:
+        load(i, p).wait()
+        store(i, p).start()
+    for i, p in order:
+        store(i, p).wait()
+
+
+def copied(results):
+    shapes = tuple(jax.ShapeDtypeStruct(r.shape, r.dtype) for r in results)
+    any_space = pl.BlockSpec(memory_space=pl.ANY)
+    sems = pltpu.SemaphoreType.DMA((len(results), HALVES))
+    return pl.pallas_call(
+        hand_over,
+        out_shape=shapes,
+        in_specs=[any_space] * len(results),
+        out_specs=(any_space,) * len(results),
+        scratch_shapes=[pltpu.VMEM(r.shape, r.dtype) for r in results] + [sems, sems],
+    )(*results)
+
+
 def make(n_fs, n_tp):
     n_x = n_tp // CORES
     n_y = n_x
@@ -551,13 +692,13 @@
         any_space = pl.BlockSpec(memory_space=pl.ANY)
         wide_grad = jax.ShapeDtypeStruct((depth, width), f32)
         flops = 2 * 8 * rows * half * model
-        input_grad, gate_grad, up_grad, down_grad = pl.pallas_call(
+        results = pl.pallas_call(
             functools.partial(kernel, n_fs, n_tp),
             out_shape=(
                 jax.ShapeDtypeStruct((tokens, part), bf16),
                 wide_grad,
                 wide_grad,
-                wide_grad,
+                jax.ShapeDtypeStruct((width, depth), f32),
             ),
             in_specs=[any_space] * 5,
             out_specs=(any_space,) * 4,
@@ -581,15 +722,15 @@
                 sem((2, 3)),
                 sem((2, 3, n_z - 2)),
                 sem((2, 3, n_z, n_y - 1)),
-                sem((2, 2)),
-                sem((2, 2, 2, n_x - 1)),
-                sem((2, 2)),
+                sem((2, 2, PIECES)),
+                sem((2, 2, 1 + PIECES, n_x - 1)),
+                sem((2, 2, 1 + PIECES)),
                 sem((2, 3, n_z, n_y - 1)),
                 sem((2, 3, n_z - 2)),
                 sem((2, 3)),
                 sem((2, 3)),
-                sem((2,)),
-                sem((2, n_x - 1)),
+                sem((2, 2)),
+                sem((2, 2, n_x - 1)),
                 sem((2,)),
             ],
             compiler_params=pltpu.CompilerParams(
@@ -598,8 +739,8 @@
             cost_estimate=pl.CostEstimate(
                 flops=flops, bytes_accessed=rows * model, transcendentals=rows * half
             ),
-        )(layer_input, out_cotangent, gate_matrix, up_matrix, down_matrix.T)
-        return input_grad, gate_grad, up_grad, down_grad.T
+        )(layer_input, out_cotangent, gate_matrix, up_matrix, down_matrix)
+        return copied(results)
 
     return on_device
 

time: 308 us -> 251 us (0.81)
  Pallas kernels: 297 us -> 248 us
  local copies, waits for them, and re-layouts: 10.2 us -> 0 us
    pallas_call x1, Pallas kernels: 297 us -> 243 us  [on_device(): pl.pallas_call(functools.partial(kernel, n_fs, n_tp), out_shape=(jax.Shap...]
    unnamed x11 -> x0, local copies, waits for them, and re-layouts: 10.2 us -> none
    pallas_call x0 -> x1, Pallas kernels: none -> 5 us  [copied(): pl.pallas_call(hand_over, out_shape=shapes, in_specs=[any_space] * len(re...]
where the time goes in v1:
time: 251 us; the launch traced here: 249 us
  Pallas kernels  248 us (99%)
    pallas_call x1, Pallas kernels, on_device(): pl.pallas_call(functools.partial(kernel, n_fs, n_tp), out_shape=(jax.Shap...  243 us

profile of v1, /device:TPU:3, one launch (start us, length us, event | category | flops | bytes accessed | tf_op | source)
XLA Modules:
  0.0 248.5 jit_solution(4965865823041329189)
XLA Ops:
  0.6 242.7 %shard_map.84 = (bf16[768,512]{1,0:T(8,128)(2,1)}, f32[256,1536]{1,0:T(8,128)}, f32[256,1536]{1,0:T(8,128)}, f32[1536,256]{1,0:T(8,128)}) custom-call(bf16[768,512]{1,0:T(8,128)(2,1)} %layer_input.1, bf16[768,512]{1,0:T(8,128)(2,1)} %out_cotangent.1, bf16[256,1536]{1,0:T(8,128)(2,1)} %gate_matrix.1, bf16[256,1536]{1,0:T(8,128)(2,1)} %up_matrix.1, ...), custom_call_target="tpu_custom_call" | custom-call | flops 38654705664 | bytes 3145728 | tf_op jit(solution)/shard_map/pallas_call | solution.py:695
  243.4 5.0 %shard_map.85 = (bf16[768,512]{1,0:T(8,128)(2,1)}, f32[256,1536]{1,0:T(8,128)}, f32[256,1536]{1,0:T(8,128)}, f32[1536,256]{1,0:T(8,128)}) custom-call(bf16[768,512]{1,0:T(8,128)(2,1)} %get-tuple-element.8.refs_0_, f32[256,1536]{1,0:T(8,128)} %get-tuple-element.9.refs_1_, f32[256,1536]{1,0:T(8,128)} %get-tuple-element.10.refs_2_, ...), custom_call_target="tpu_custom_call" | custom-call | tf_op jit(solution)/shard_map/pallas_call | solution.py:669

commit v2 on v1

--- a/solution.py
+++ b/solution.py
@@ -60,6 +60,7 @@
     y_out,
     y_in,
     far_in,
+    direct_in,
     near_in,
     core_in,
     dx_out,
@@ -71,12 +72,14 @@
     ag_core,
     ag_near,
     ag_far,
+    ag_direct,
     ag_y,
     tok_z,
     tok_x,
     tok_core,
     rs_y,
     rs_far,
+    rs_direct,
     rs_near,
     rs_core,
     dx_core_sem,
@@ -142,6 +145,7 @@
     partners = (
         [at_core, at_z(1)]
         + [at_z(e) for e in far]
+        + [at_z(3)]
         + [at_y(d) for d in range(1, n_y)]
         + [at_x(d) for d in range(1, n_x)]
     )
@@ -149,6 +153,10 @@
         pl.semaphore_signal(
             barrier, inc=1, device_id=partner, device_id_type=pl.DeviceIdType.MESH
         )
+
+    outer = lax.div(jnp.abs(2 * z - (n_z - 1)), n_z - 1)
+    at_ends = pl.when(outer == 1)
+    at_inner = pl.when(outer == 0)
 
     shards = (gate_matrix, up_matrix)
     sources = (layer_input, out_cotangent)
@@ -196,6 +204,11 @@
             w.at[m, pl.ds(model, depth), :], w.at[m, span(here, depth), :], ag_near, (m,), at_z(1)
         )
 
+    def direct_shard(m):
+        return remote(
+            w.at[m, pl.ds(model, depth), :], w.at[m, span(here, depth), :], ag_direct, (m,), at_z(3)
+        )
+
     def far_shard(m, e, s):
         block = w.at[m, span(first(place(s, 0)), depth), :]
         return remote(block, block, ag_far, (m, e - 2 + s), at_z(e))
@@ -249,19 +262,27 @@
 
     def relay_near(m):
         near_shard(m).wait_recv()
-        for e in far:
-            far_shard(m, e, 1).start()
+
+        @at_inner
+        def _():
+            far_shard(m, 2, 1).start()
+
         send_y_shards(m, 1)
 
-    def relay_far(m, s):
-        for e in far:
-            far_shard(m, e, s).wait_recv()
-            send_y_shards(m, e + s)
-
-    def start_last():
-        for h in range(PIECES):
-            token_z(1, h).start()
-        near_shard(DOWN).start()
+    def relay_far(m):
+        far_shard(m, 2, 0).wait_recv()
+        send_y_shards(m, 2)
+
+    def relay_last(m):
+        @at_inner
+        def _():
+            direct_shard(m).wait_recv()
+
+        @at_ends
+        def _():
+            far_shard(m, 2, 1).wait_recv()
+
+        send_y_shards(m, 3)
 
 
     def send_y_shards(m, zr):
@@ -288,44 +309,54 @@
     for h in range(PIECES):
         token_z(0, h).start()
     for m in (GATE, UP):
-        for e in far:
-            far_shard(m, e, 0).start()
+        far_shard(m, 2, 0).start()
+
+    @at_ends
+    def _():
+        direct_in[...] = jnp.zeros_like(direct_in)
+        far_in[:, 1] = jnp.zeros((3, depth, half), far_in.dtype)
+
     turn_down()
     swap_shard(DOWN).start()
     swap_shard(DOWN).wait_recv()
     send_y_shards(DOWN, 0)
-    outer = lax.div(jnp.abs(2 * z - (n_z - 1)), n_z - 1)
-
-    @pl.when(outer == 0)
+    @at_inner
     def _():
         for m in (GATE, UP):
             relay_near(m)
-        start_last()
+        for m in (GATE, UP):
+            direct_shard(m).start()
+        for h in range(PIECES):
+            token_z(1, h).start()
+        near_shard(DOWN).start()
         for h in range(PIECES):
             pass_tokens(0, h)
         for m in (GATE, UP):
-            relay_far(m, 0)
+            relay_far(m)
         for p in range(1 + PIECES):
             join_tokens(0, p)
+        far_shard(DOWN, 2, 0).start()
         for m in (GATE, UP):
-            relay_far(m, 1)
-
-    @pl.when(outer == 1)
+            relay_last(m)
+        relay_near(DOWN)
+        direct_shard(DOWN).start()
+
+    @at_ends
     def _():
+        near_shard(DOWN).start()
+        for h in range(PIECES):
+            token_z(1, h).start()
+        far_shard(DOWN, 2, 0).start()
         for m in (GATE, UP):
-            relay_far(m, 0)
+            relay_far(m)
+        for m in (GATE, UP):
+            relay_last(m)
         for m in (GATE, UP):
             relay_near(m)
-        for m in (GATE, UP):
-            relay_far(m, 1)
-        start_last()
         for h in range(PIECES):
             pass_tokens(0, h)
             join_tokens(0, h)
         join_tokens(0, PIECES)
-
-    for e in far:
-        far_shard(DOWN, e, 0).start()
 
     def arrived(m):
         for zr in range(n_z):
@@ -361,13 +392,23 @@
         pass_tokens(1, h)
         join_tokens(1, h)
         if h == 0:
-
-            @pl.when(outer == 1)
+            relay_far(DOWN)
+        elif h == 1:
+
+            @at_ends
             def _():
-                relay_far(DOWN, 0)
-
-    relay_near(DOWN)
+                relay_last(DOWN)
+
+    @at_ends
+    def _():
+        relay_near(DOWN)
+
     join_tokens(1, PIECES)
+
+    @at_inner
+    def _():
+        relay_last(DOWN)
+
     await_tokens(1)
 
     def term(m, zr, yr):
@@ -382,6 +423,9 @@
 
     def far_sum(m, zr, e):
         return remote(y_out.at[m, zr, 0], far_in.at[m, zr - 2], rs_far, (m, zr - 2), at_z(e))
+
+    def direct_sum(m):
+        return remote(y_out.at[m, 3, 0], direct_in.at[m], rs_direct, (m,), at_z(3))
 
     def near_sum(m):
         return remote(y_out.at[m, 1, 0], near_in.at[m], rs_near, (m,), at_z(1))
@@ -404,14 +448,26 @@
 
     def cross(m, zr, e):
         y_out[m, zr, 0] = narrow(y_sum(m, zr))
-        far_sum(m, zr, e).start()
+        if zr != 3:
+            far_sum(m, zr, e).start()
+            return
+
+        @at_inner
+        def _():
+            direct_sum(m).start()
+
+        @at_ends
+        def _():
+            far_sum(m, 3, 2).start()
 
     def pair(m):
         total = y_sum(m, 1)
-        for e in far:
-            far_sum(m, e + 1, e).wait_recv()
-            total = total + wide(far_in[m, e - 1])
-        y_out[m, 1, 0] = narrow(total)
+
+        @at_inner
+        def _():
+            far_sum(m, 3, 2).wait_recv()
+
+        y_out[m, 1, 0] = narrow(total + wide(far_in[m, 1]))
         near_sum(m).start()
 
     def own_stage(m):
@@ -426,7 +482,12 @@
             far_sum(m, e, e).wait_recv()
             total = total + wide(far_in[m, e - 2])
         near_sum(m).wait_recv()
-        other = wide(near_in[m])
+
+        @at_inner
+        def _():
+            direct_sum(m).wait_recv()
+
+        other = wide(near_in[m]) + wide(direct_in[m])
         y_out[m, 0, 0] = narrow(jnp.where(mine == 1, other, total))
         core_sum(m).start()
         kept = jnp.where(mine == 1, total, other)
@@ -458,25 +519,9 @@
         for copy in put(m):
             copy.start()
 
-    send_y(DOWN, 3)
-
-    @pl.when(outer == 0)
-    def _():
-        relay_far(DOWN, 0)
-        relay_far(DOWN, 1)
-
-    @pl.when(outer == 1)
-    def _():
-        cross(DOWN, 3, 2)
-        relay_far(DOWN, 1)
-
-    @pl.loop(0, 2)
+    @pl.loop(0, 3)
     def _(i):
-        send_y(DOWN, 2 - i)
-
-    @pl.when(outer == 0)
-    def _():
-        cross(DOWN, 3, 2)
+        send_y(DOWN, 3 - i)
 
     arrived(DOWN)
 
@@ -561,6 +606,7 @@
             send_y(m, zr)
 
     dx_give(1)
+    cross(DOWN, 3, 2)
     send_pair(3)
     cross(DOWN, 2, 2)
     dx_take(1)
@@ -623,10 +669,19 @@
         near_shard(m).wait_send()
         near_sum(m).wait_send()
         core_sum(m).wait_send()
-        for e in far:
-            for s in range(2):
-                far_shard(m, e, s).wait_send()
-                far_sum(m, e + s, e).wait_send()
+        far_shard(m, 2, 0).wait_send()
+        far_sum(m, 2, 2).wait_send()
+
+        @at_inner
+        def _():
+            far_shard(m, 2, 1).wait_send()
+            direct_shard(m).wait_send()
+            direct_sum(m).wait_send()
+
+        @at_ends
+        def _():
+            far_sum(m, 3, 2).wait_send()
+
         for zr in range(n_z):
             for yr in range(1, n_y):
                 y_shard(m, zr, yr).wait_send()
@@ -712,6 +767,7 @@
                 pltpu.VMEM((3, n_z - 2, depth, half), bf16),
                 pltpu.VMEM((3, depth, half), bf16),
                 pltpu.VMEM((3, depth, half), bf16),
+                pltpu.VMEM((3, depth, half), bf16),
                 pltpu.VMEM((rows, near), bf16),
                 pltpu.VMEM((rows, near), bf16),
                 pltpu.VMEM((n_x - 1, rows, part), bf16),
@@ -721,12 +777,14 @@
                 sem((2, 3)),
                 sem((2, 3)),
                 sem((2, 3, n_z - 2)),
+                sem((2, 3)),
                 sem((2, 3, n_z, n_y - 1)),
                 sem((2, 2, PIECES)),
                 sem((2, 2, 1 + PIECES, n_x - 1)),
                 sem((2, 2, 1 + PIECES)),
                 sem((2, 3, n_z, n_y - 1)),
                 sem((2, 3, n_z - 2)),
+                sem((2, 3)),
                 sem((2, 3)),
                 sem((2, 3)),
                 sem((2, 2)),

time: 251 us -> 243 us (0.968)
  Pallas kernels: 248 us -> 242 us
    pallas_call x1, Pallas kernels: 243 us -> 237 us  [on_device(): pl.pallas_call(functools.partial(kernel, n_fs, n_tp), out_shape=(jax.Shap...]
where the time goes in v2:
time: 243 us
  Pallas kernels  242 us (100%)
    pallas_call x1, Pallas kernels, on_device(): pl.pallas_call(functools.partial(kernel, n_fs, n_tp), out_shape=(jax.Shap...  237 us
    pallas_call x1, Pallas kernels, copied(): pl.pallas_call(hand_over, out_shape=shapes, in_specs=[any_space] * len(re...  5 us

profile of v2, /device:TPU:3, one launch (start us, length us, event | category | flops | bytes accessed | tf_op | source)
XLA Modules:
  0.0 242.8 jit_solution(18334457332096468500)
XLA Ops:
  0.6 237.0 %shard_map.84 = (bf16[768,512]{1,0:T(8,128)(2,1)}, f32[256,1536]{1,0:T(8,128)}, f32[256,1536]{1,0:T(8,128)}, f32[1536,256]{1,0:T(8,128)}) custom-call(bf16[768,512]{1,0:T(8,128)(2,1)} %layer_input.1, bf16[768,512]{1,0:T(8,128)(2,1)} %out_cotangent.1, bf16[256,1536]{1,0:T(8,128)(2,1)} %gate_matrix.1, bf16[256,1536]{1,0:T(8,128)(2,1)} %up_matrix.1, ...), custom_call_target="tpu_custom_call" | custom-call | flops 38654705664 | bytes 3145728 | tf_op jit(solution)/shard_map/pallas_call | solution.py:750
  237.7 5.0 %shard_map.85 = (bf16[768,512]{1,0:T(8,128)(2,1)}, f32[256,1536]{1,0:T(8,128)}, f32[256,1536]{1,0:T(8,128)}, f32[1536,256]{1,0:T(8,128)}) custom-call(bf16[768,512]{1,0:T(8,128)(2,1)} %get-tuple-element.8.refs_0_, f32[256,1536]{1,0:T(8,128)} %get-tuple-element.9.refs_1_, f32[256,1536]{1,0:T(8,128)} %get-tuple-element.10.refs_2_, ...), custom_call_target="tpu_custom_call" | custom-call | tf_op jit(solution)/shard_map/pallas_call | solution.py:724

commit v3 on v2

--- a/solution.py
+++ b/solution.py
@@ -644,11 +644,8 @@
     own(DOWN)
     finish(DOWN)
 
-    @pl.loop(0, 2)
-    def _(m):
+    for m in (GATE, UP):
         own(m)
-
-    for m in (GATE, UP):
         finish(m)
 
     dx_over_z.wait_send()

time: 243 us -> 243 us (level)
  no operation moved by 1% of the time
where the time goes in v3:
time: 243 us
  Pallas kernels  242 us (100%)
    pallas_call x1, Pallas kernels, on_device(): pl.pallas_call(functools.partial(kernel, n_fs, n_tp), out_shape=(jax.Shap...  237 us
    pallas_call x1, Pallas kernels, copied(): pl.pallas_call(hand_over, out_shape=shapes, in_specs=[any_space] * len(re...  5 us

profile of v3, /device:TPU:3, one launch (start us, length us, event | category | flops | bytes accessed | tf_op | source)
XLA Modules:
  0.0 242.9 jit_solution(12613628430711830733)
XLA Ops:
  0.6 237.0 %shard_map.84 = (bf16[768,512]{1,0:T(8,128)(2,1)}, f32[256,1536]{1,0:T(8,128)}, f32[256,1536]{1,0:T(8,128)}, f32[1536,256]{1,0:T(8,128)}) custom-call(bf16[768,512]{1,0:T(8,128)(2,1)} %layer_input.1, bf16[768,512]{1,0:T(8,128)(2,1)} %out_cotangent.1, bf16[256,1536]{1,0:T(8,128)(2,1)} %gate_matrix.1, bf16[256,1536]{1,0:T(8,128)(2,1)} %up_matrix.1, ...), custom_call_target="tpu_custom_call" | custom-call | flops 38654705664 | bytes 3145728 | tf_op jit(solution)/shard_map/pallas_call | solution.py:747
  237.7 5.0 %shard_map.85 = (bf16[768,512]{1,0:T(8,128)(2,1)}, f32[256,1536]{1,0:T(8,128)}, f32[256,1536]{1,0:T(8,128)}, f32[1536,256]{1,0:T(8,128)}) custom-call(bf16[768,512]{1,0:T(8,128)(2,1)} %get-tuple-element.8.refs_0_, f32[256,1536]{1,0:T(8,128)} %get-tuple-element.9.refs_1_, f32[256,1536]{1,0:T(8,128)} %get-tuple-element.10.refs_2_, ...), custom_call_target="tpu_custom_call" | custom-call | tf_op jit(solution)/shard_map/pallas_call | solution.py:721
